TPU v7x, 256 devices: a whole 4x4x8 slice. The times are simulated.
256 devices in a mesh: kv: 32 (over z, y), tp: 8 (over x, core).
Axes of the slice: x: 4, y: 4, z: 8, core: 2. Of those that a mesh axis runs over, the one named last changes fastest.
Arguments:
- tokens: bfloat16 [16, 4096], P(None, ('kv', 'tp')), may hold values from -17 to 17
- first_gain: float32 [4096], P('kv'), may hold values from 0.1 to 1.9
- first_gate: bfloat16 [4096, 11264], P('kv', 'tp'), may hold values from -0.09375 to 0.09375
- first_up: bfloat16 [4096, 11264], P('kv', 'tp'), may hold values from -0.09375 to 0.09375
- first_down: bfloat16 [11264, 4096], P('tp', 'kv'), may hold values from -0.0546875 to 0.0546875
- mixer_gain: float32 [4096], P('kv'), may hold values from 0.1 to 1.9
- w_query: bfloat16 [4096, 4096], P('kv', 'tp'), may hold values from -0.09375 to 0.09375
- w_key: bfloat16 [4096, 4096], P('kv', 'tp'), may hold values from -0.328125 to 0.328125
- w_value: bfloat16 [4096, 4096], P('kv', 'tp'), may hold values from -0.09375 to 0.09375
- w_output: bfloat16 [4096, 4096], P('tp', 'kv'), may hold values from -0.09375 to 0.09375
- lam_heads: float32 [32], P('tp'), may hold values from 0.3 to 0.8
- head_gain: float32 [128], replicated, may hold values from 0.1 to 1.9
- key_cache: bfloat16 [16, 8192, 32, 128], P(None, 'kv', 'tp'), may hold values from -1000 to 1000
- value_cache: bfloat16 [16, 8192, 32, 128], P(None, 'kv', 'tp'), may hold values from -6 to 6
- lengths: int32 [16], replicated, may hold values from 1 to 8192, 49152 in all
- last_gain: float32 [4096], P('kv'), may hold values from 0.1 to 1.9
- last_gate: bfloat16 [4096, 11264], P('kv', 'tp'), may hold values from -0.09375 to 0.09375
- last_up: bfloat16 [4096, 11264], P('kv', 'tp'), may hold values from -0.09375 to 0.09375
- last_down: bfloat16 [11264, 4096], P('tp', 'kv'), may hold values from -0.0546875 to 0.0546875
Outputs:
- result: bfloat16 [16, 4096], P(None, ('kv', 'tp'))
Inputs may be any that keep to these rules, and one draw needn't show every extreme that they name: Sequence b reads cached positions 0 to lengths[b] - 1 and its new token.
All inputs are finite; a program needn't handle non-finite values.
Results may differ from a plain program's by a relative error of at most 0.04.
Values may be sent and summed in bfloat16 or wider, within the bound.
A program may use at most 64 MiB of HBM per device.

v0:
```python
import functools

import jax
import jax.numpy as jnp
from jax import lax
from jax.sharding import Mesh
from jax.sharding import PartitionSpec as P

WIDTH = 4096
HEAD_DIM = 64
VAL_DIM = 128
KV = ("kv_0", "kv_1")
KV_TP = ("kv_0", "kv_1", "tp")


epsilon = 1e-06
neg_fill = -1e30


def sent_to_all(array, axis):
    copies = jnp.broadcast_to(array, (lax.axis_size(axis), *array.shape))
    return lax.all_to_all(copies, axis, split_axis=0, concat_axis=0, tiled=True)


def laid_out(tiles, dim):
    tiles = jnp.moveaxis(tiles, 0, dim)
    shape = tiles.shape
    return tiles.reshape(*shape[:dim], shape[dim] * shape[dim + 1], *shape[dim + 2 :])


def gather_directly(array, axis, dim):
    tiles = sent_to_all(array, axis)
    return laid_out(tiles, dim)


def one_axis_at_a_time(array, axes):
    return functools.reduce(lax.psum, axes, array)


def in_blocks(array, dim, devices):
    shape = array.shape
    tiles = array.reshape(*shape[:dim], devices, shape[dim] // devices, *shape[dim + 1 :])
    return jnp.moveaxis(tiles, dim, 0)


def sent_and_summed(array, axis, dim):
    tiles = in_blocks(array, dim, lax.axis_size(axis))
    arrived = lax.all_to_all(tiles, axis, split_axis=0, concat_axis=0, tiled=True)
    return arrived.sum(axis=0)


def of_everyone(array, axis):
    return sent_to_all(array, axis).astype(jnp.float32).sum(axis=0)


def all_in_one(array, axis):
    leaves = jax.tree.leaves(array)
    turns = sorted(range(len(leaves)), key=lambda k: -leaves[k].size)
    width = (1, *leaves[turns[0]].shape)[-1]
    lines = [
        jnp.pad(leaves[k].reshape(-1), (0, -leaves[k].size % width)).reshape(-1, width)
        for k in turns
    ]
    both, at, found = (lax.all_gather(jnp.concatenate(lines), axis), 0, {})
    for k, line in zip(turns, lines):
        section = both[:, at : at + len(line)].reshape(len(both), -1)
        found[k] = section[:, : leaves[k].size].reshape(-1, *leaves[k].shape)
        at += len(line)
    numbers = iter(range(len(leaves)))
    return jax.tree.map(lambda _: found[next(numbers)], array)


def combined_by_axis(array, axes, combine):
    for axis in axes:
        pieces = all_in_one(
            jax.tree.map(
                lambda part, kind: part.astype(kind),
                array,
                (jnp.bfloat16, jnp.bfloat16, jnp.bfloat16),
            ),
            axis,
        )
        widened = [
            jax.tree.map(lambda part, own: part[k].astype(own.dtype), pieces, array)
            for k in range(lax.axis_size(axis))
        ]
        array = widened[0]
        for received in widened[1:]:
            array = combine(array, received)
    return array


def norm_block(stream_cols, gain):
    gathered = gather_directly(stream_cols, "tp", 1)
    wide = gathered.astype(jnp.float32)
    squares = jnp.sum(wide * wide, axis=1, keepdims=True)
    scaled = (wide * gain).astype(jnp.bfloat16)
    return (squares, scaled)


def gated_units(stream_cols, gain, gate_w, up_w, down_w):
    squares, scaled = norm_block(stream_cols, gain)
    part_gate = jnp.dot(scaled, gate_w, preferred_element_type=jnp.float32)
    part_up = jnp.dot(scaled, up_w, preferred_element_type=jnp.float32)
    gate_sum, up_sum, total_sq = (
        one_axis_at_a_time(part_gate.astype(jnp.bfloat16), KV).astype(jnp.float32),
        one_axis_at_a_time(part_up.astype(jnp.bfloat16), KV).astype(jnp.float32),
        one_axis_at_a_time(squares.astype(jnp.bfloat16), KV).astype(jnp.float32),
    )
    inv_rms = lax.rsqrt(total_sq / WIDTH + epsilon)
    hidden_act = (jax.nn.silu(gate_sum * inv_rms) * (up_sum * inv_rms)).astype(jnp.bfloat16)
    part_down = jnp.dot(hidden_act, down_w, preferred_element_type=jnp.float32)
    return sent_and_summed(part_down, "tp", 1)


def merge_parts(earlier, later):
    peak_one, sum_one, acc_one = earlier
    peak_two, sum_two, acc_two = later
    highest = jnp.maximum(peak_one, peak_two)
    scale_one = jnp.exp(peak_one - highest)
    scale_two = jnp.exp(peak_two - highest)
    return (
        highest,
        scale_one * sum_one + scale_two * sum_two,
        scale_one[..., None] * acc_one + scale_two[..., None] * acc_two,
    )


def attend(
    stream_cols,
    mixer_gain,
    w_query,
    w_key,
    w_value,
    w_output,
    lam_heads,
    head_gain,
    key_cache,
    value_cache,
    lengths,
):
    squares, scaled = norm_block(stream_cols, mixer_gain)
    part_query = jnp.dot(scaled, w_query, preferred_element_type=jnp.float32)
    part_key = jnp.dot(scaled, w_key, preferred_element_type=jnp.float32)
    part_value = jnp.dot(scaled, w_value, preferred_element_type=jnp.float32)
    query_sum, key_sum, value_sum, total_sq = (
        of_everyone(part_query.astype(jnp.bfloat16), KV).astype(jnp.float32),
        of_everyone(part_key.astype(jnp.bfloat16), KV).astype(jnp.float32),
        of_everyone(part_value.astype(jnp.bfloat16), KV).astype(jnp.float32),
        of_everyone(squares.astype(jnp.bfloat16), KV).astype(jnp.float32),
    )
    inv_rms = lax.rsqrt(total_sq / WIDTH + epsilon)
    rows_count = scaled.shape[0]
    shard_heads = key_cache.shape[2]
    local_pos = key_cache.shape[1]
    logit_scale = HEAD_DIM ** (-0.5)
    query_rows = (
        (query_sum * inv_rms).astype(jnp.bfloat16).reshape(rows_count, shard_heads, 2, HEAD_DIM)
    )
    fresh_key = (
        (key_sum * inv_rms).astype(jnp.bfloat16).reshape(rows_count, shard_heads, 2, HEAD_DIM)
    )
    new_value = (value_sum * inv_rms).astype(jnp.bfloat16).reshape(rows_count, shard_heads, VAL_DIM)
    offset = lax.axis_index(KV) * local_pos
    positions = offset + jnp.arange(local_pos, dtype=jnp.int32)
    live_mask = (positions[None, :] < lengths[:, None])[:, None, None, :]
    key_entries = key_cache.reshape(rows_count, local_pos, shard_heads, 2, HEAD_DIM)
    score_matrix = (
        jnp.einsum("bhmd,bphmd->bhmp", query_rows, key_entries, preferred_element_type=jnp.float32)
        * logit_scale
    )
    score_matrix = jnp.where(live_mask, score_matrix, neg_fill)
    peak_score = jnp.max(score_matrix, axis=-1)
    weights = jnp.where(live_mask, jnp.exp(score_matrix - peak_score[..., None]), 0.0)
    totals = jnp.sum(weights, axis=-1)
    weighted = jnp.einsum(
        "bhmp,bphe->bhme",
        weights.astype(jnp.bfloat16),
        value_cache,
        preferred_element_type=jnp.float32,
    )
    peak_score, totals, weighted = combined_by_axis((peak_score, totals, weighted), KV, merge_parts)
    self_score = (
        jnp.sum(query_rows.astype(jnp.float32) * fresh_key.astype(jnp.float32), axis=-1)
        * logit_scale
    )
    highest = jnp.maximum(peak_score, self_score)
    scale_old = jnp.exp(peak_score - highest)
    own_weight = jnp.exp(self_score - highest)
    own_round = lax.optimization_barrier(own_weight.astype(jnp.bfloat16)).astype(jnp.float32)
    totals = scale_old * totals + own_weight
    weighted = (
        scale_old[..., None] * weighted
        + own_round[..., None] * new_value.astype(jnp.float32)[:, :, None, :]
    )
    mixed = (
        weighted[:, :, 0] / totals[:, :, 0, None]
        - lam_heads[None, :, None] * weighted[:, :, 1] / totals[:, :, 1, None]
    )
    normed = (
        mixed * lax.rsqrt(jnp.mean(mixed * mixed, axis=-1, keepdims=True) + epsilon) * head_gain
    )
    attended = normed.astype(jnp.bfloat16).reshape(rows_count, shard_heads * VAL_DIM)
    part_out = jnp.dot(attended, w_output, preferred_element_type=jnp.float32)
    return sent_and_summed(part_out, "tp", 1)


def on_device(
    tokens,
    first_gain,
    first_gate,
    first_up,
    first_down,
    mixer_gain,
    w_query,
    w_key,
    w_value,
    w_output,
    lam_heads,
    head_gain,
    key_cache,
    value_cache,
    lengths,
    last_gain,
    last_gate,
    last_up,
    last_down,
):
    first_branch = gated_units(tokens, first_gain, first_gate, first_up, first_down)
    first = (tokens.astype(jnp.float32) + 0.5 * first_branch).astype(jnp.bfloat16)
    projected = attend(
        first,
        mixer_gain,
        w_query,
        w_key,
        w_value,
        w_output,
        lam_heads,
        head_gain,
        key_cache,
        value_cache,
        lengths,
    )
    second = (first.astype(jnp.float32) + projected).astype(jnp.bfloat16)
    last_branch = gated_units(second, last_gain, last_gate, last_up, last_down)
    return (second.astype(jnp.float32) + 0.5 * last_branch).astype(jnp.bfloat16)


def solution(mesh):
    finer = Mesh(mesh.devices.reshape(8, 4, mesh.shape["tp"]), ("kv_0", "kv_1", "tp"))
    return jax.shard_map(
        on_device,
        mesh=finer,
        in_specs=(
            P(None, KV_TP),
            P(KV),
            P(KV, "tp"),
            P(KV, "tp"),
            P("tp", KV),
            P(KV),
            P(KV, "tp"),
            P(KV, "tp"),
            P(KV, "tp"),
            P("tp", KV),
            P("tp"),
            P(),
            P(None, KV, "tp", None),
            P(None, KV, "tp", None),
            P(),
            P(KV),
            P(KV, "tp"),
            P(KV, "tp"),
            P("tp", KV),
        ),
        out_specs=P(None, KV_TP),
        check_vma=False,
    )
```

profile of v0, /device:TPU:1, one launch (start us, length us, event | category | flops | bytes accessed | tf_op | source)
XLA Modules:
  0.0 436.8 jit_solution(5309866430094227475)
XLA Ops:
  6.5 0.7 broadcast_in_dim.32
  7.4 10.2 %all_to_all.50 = bf16[8,2,128]{2,1,0:T(2,128)(2,1)S(1)} all-to-all(bf16[8,2,128]{2,1,0:T(2,128)(2,1)S(1)} %reshape.1266), channel_id=1, replica_groups=mesh['kv_0'=8,'kv_1'=4,'tp'=8] {'tp'}, dimensions={0} | all-to-all | bytes 8192 | tf_op jit(solution)/shard_map/all_to_all | solution.py:22
  17.7 0.6 fusion.6
  18.4 1.4 convolution_convert_fusion.2
  19.8 1.8 convolution_convert_fusion.3
  21.7 68.7 %all-reduce.11.cloned.1.call-done = (bf16[16,1408]{1,0:T(8,128)(2,1)}, bf16[16,1408]{1,0:T(8,128)(2,1)}, bf16[16,1]{0,1:T(2,128)(2,1)}) async-done(((bf16[16,1408]{1,0:T(8,128)(2,1)}, bf16[16,1408]{1,0:T(8,128)(2,1)}, bf16[16,1]{0,1:T(2,128)(2,1)}), (bf16[16,1408]{1,0:T(8,128)(2,1)}, bf16[16,1408]{1,0:T(8,128)(2,1)}, bf16[16,1]{0,1:T(2,128)(2,1)})) %all-reduce.11.cloned.1.call-update) | async-done | bytes 90160 | tf_op jit(solution)/shard_map/psum | solution.py:37
  90.4 50.1 %all-reduce.15.cloned.1.call-done = (bf16[16,1408]{1,0:T(8,128)(2,1)}, bf16[16,1408]{1,0:T(8,128)(2,1)}, bf16[16,1]{0,1:T(2,128)(2,1)}) async-done(((bf16[16,1408]{1,0:T(8,128)(2,1)}, bf16[16,1408]{1,0:T(8,128)(2,1)}, bf16[16,1]{0,1:T(2,128)(2,1)}), (bf16[16,1408]{1,0:T(8,128)(2,1)}, bf16[16,1408]{1,0:T(8,128)(2,1)}, bf16[16,1]{0,1:T(2,128)(2,1)})) %all-reduce.15.cloned.1.call-update) | async-done | bytes 90160 | tf_op jit(solution)/shard_map/psum | solution.py:37
  140.5 0.6 rsqrt_bitcast_fusion.1
  141.2 1.3 fusion.35
  142.7 11.5 %all_to_all.51 = f32[8,1,256]{2,1,0:T(1,128)S(1)} all-to-all(f32[8,1,256]{2,1,0:T(1,128)S(1)} %reshape.1268), channel_id=1, replica_groups=mesh['kv_0'=8,'kv_1'=4,'tp'=8] {'tp'}, dimensions={0} | all-to-all | bytes 16384 | tf_op jit(solution)/shard_map/all_to_all | solution.py:48
  154.1 0.5 broadcast.199
  154.6 0.7 reduce.39
  155.4 0.7 add_convert_fusion.2
  156.2 7.6 %all_to_all.52 = bf16[8,2,128]{2,1,0:T(2,128)(2,1)S(1)} all-to-all(bf16[8,2,128]{2,1,0:T(2,128)(2,1)S(1)} %reshape.1270), channel_id=1, replica_groups=mesh['kv_0'=8,'kv_1'=4,'tp'=8] {'tp'}, dimensions={0} | all-to-all | bytes 8192 | tf_op jit(solution)/shard_map/all_to_all | solution.py:22
  164.2 0.6 broadcast_in_dim.36
  164.8 8.1 %all-to-all-start.4 = ((bf16[32,16,1]{1,2,0:T(2,128)(2,1)}), bf16[32,16,1]{1,2,0:T(2,128)(2,1)S(1)}, u32[]{:S(2)}, u32[]{:S(2)}) async-start(bf16[32,16,1]{1,2,0:T(2,128)(2,1)} %broadcast_in_dim.36), calls=%async_computation.4 | async-start | bytes 32768 | tf_op jit(solution)/shard_map/all_to_all | solution.py:22
  172.9 0.7 multiply_convert_fusion.7
  173.6 1.0 convolution_convert_fusion.6
  174.6 6.9 %all-to-all-done.4 = bf16[32,16,1]{1,2,0:T(2,128)(2,1)S(1)} async-done(((bf16[32,16,1]{1,2,0:T(2,128)(2,1)}), bf16[32,16,1]{1,2,0:T(2,128)(2,1)S(1)}, u32[]{:S(2)}, u32[]{:S(2)}) %all-to-all-start.4) | async-done | bytes 1056 | tf_op jit(solution)/shard_map/all_to_all | solution.py:22
  181.6 0.9 broadcast_in_dim.35
  182.4 3.9 all-to-all-start.3
  186.4 7.4 %copy.85 = bf16[16,256,4,128]{1,3,2,0:T(8,128)(2,1)} copy(bf16[16,256,4,128]{3,2,1,0:T(4,128)(2,1)} %param.31) | data formatting | bytes 8388608 | tf_op args[12]
  193.9 0.1 convolution_convert_fusion.5
  194.0 7.3 %all-to-all-done.3 = bf16[32,16,512]{2,1,0:T(8,128)(2,1)S(1)} async-done(((bf16[32,16,512]{2,1,0:T(8,128)(2,1)}), bf16[32,16,512]{2,1,0:T(8,128)(2,1)S(1)}, u32[]{:S(2)}, u32[]{:S(2)}) %all-to-all-start.3) | async-done | bytes 524320 | tf_op jit(solution)/shard_map/all_to_all | solution.py:22
  201.3 0.9 broadcast_in_dim.39
  202.2 6.2 %all-to-all-start.5 = ((bf16[32,16,512]{2,1,0:T(8,128)(2,1)}), bf16[32,16,512]{2,1,0:T(8,128)(2,1)S(1)}, u32[]{:S(2)}, u32[]{:S(2)}) async-start(bf16[32,16,512]{2,1,0:T(8,128)(2,1)} %broadcast_in_dim.39), calls=%async_computation.5 | async-start | bytes 1048576 | tf_op jit(solution)/shard_map/all_to_all | solution.py:22
  208.5 0.1 convolution_convert_fusion.4
  208.9 14.5 %all-to-all-done.5 = bf16[32,16,512]{2,1,0:T(8,128)(2,1)S(1)} async-done(((bf16[32,16,512]{2,1,0:T(8,128)(2,1)}), bf16[32,16,512]{2,1,0:T(8,128)(2,1)S(1)}, u32[]{:S(2)}, u32[]{:S(2)}) %all-to-all-start.5) | async-done | bytes 524320 | tf_op jit(solution)/shard_map/all_to_all | solution.py:22
  223.4 0.9 broadcast_in_dim.40
  224.2 6.3 %all-to-all-start.6 = ((bf16[32,16,512]{2,1,0:T(8,128)(2,1)}), bf16[32,16,512]{2,1,0:T(8,128)(2,1)S(1)}, u32[]{:S(2)}, u32[]{:S(2)}) async-start(bf16[32,16,512]{2,1,0:T(8,128)(2,1)} %broadcast_in_dim.40), calls=%async_computation.6 | async-start | bytes 1048576 | tf_op jit(solution)/shard_map/all_to_all | solution.py:22
  230.8 0.2 multiply_reduce_fusion
  231.0 3.0 fusion.30
  234.0 0.2 fusion.41
  234.2 0.3 fusion.105
  234.6 0.7 fusion.2
  235.3 0.2 convert_element_type.988
  235.5 0.1 convert_element_type.986
  235.6 22.2 %all-gather.2 = bf16[8,130,128]{2,1,0:T(8,128)(2,1)S(1)} all-gather(bf16[1,130,128]{2,1,0:T(8,128)(2,1)S(1)} %maximum_bitcast_fusion), channel_id=2, replica_groups=mesh['kv_0'=8,'kv_1'=4,'tp'=8] {'kv_0'}, dimensions={0}, use_global_device_ids=true | all-gather | bytes 299520 | tf_op jit(solution)/shard_map/all_gather | solution.py:64
  257.9 0.3 fusion.17
  258.2 9.5 %all-gather.3 = bf16[4,130,128]{2,1,0:T(8,128)(2,1)S(1)} all-gather(bf16[1,130,128]{2,1,0:T(8,128)(2,1)S(1)} %maximum_bitcast_fusion.1), channel_id=3, replica_groups=mesh['kv_0'=8,'kv_1'=4,'tp'=8] {'kv_1'}, dimensions={0}, use_global_device_ids=true | all-gather | bytes 166400 | tf_op jit(solution)/shard_map/all_gather | solution.py:64
  267.8 0.2 reshape.1207
  268.1 0.2 reshape.1208
  268.3 0.2 reshape.1209
  268.6 0.2 reshape.1210
  268.9 0.2 reshape.1199
  269.2 0.2 reshape.1200
  269.4 0.2 reshape.1201
  269.7 0.2 reshape.1202
  271.1 0.6 fusion.11
  272.0 0.2 multiply_reduce_fusion.1
  272.3 0.2 convolution_bitcast_fusion
  272.7 17.1 %all_to_all.53 = f32[8,1,256]{2,1,0:T(1,128)S(1)} all-to-all(f32[8,1,256]{2,1,0:T(1,128)S(1)} %reshape.1272), channel_id=1, replica_groups=mesh['kv_0'=8,'kv_1'=4,'tp'=8] {'tp'}, dimensions={0} | all-to-all | bytes 16384 | tf_op jit(solution)/shard_map/all_to_all | solution.py:48
  289.8 0.7 reduce.40
  290.7 7.6 %all_to_all.54 = bf16[8,2,128]{2,1,0:T(2,128)(2,1)S(1)} all-to-all(bf16[8,2,128]{2,1,0:T(2,128)(2,1)S(1)} %reshape.1274), channel_id=1, replica_groups=mesh['kv_0'=8,'kv_1'=4,'tp'=8] {'tp'}, dimensions={0} | all-to-all | bytes 8192 | tf_op jit(solution)/shard_map/all_to_all | solution.py:22
  298.4 0.7 fusion.8
  299.2 0.8 convolution_convert_fusion
  300.0 0.8 convolution_convert_fusion.1
  300.8 64.7 %all-reduce.9.cloned.1.call-done = (bf16[16,1408]{1,0:T(8,128)(2,1)}, bf16[16,1408]{1,0:T(8,128)(2,1)}, bf16[16,1]{0,1:T(2,128)(2,1)}) async-done(((bf16[16,1408]{1,0:T(8,128)(2,1)}, bf16[16,1408]{1,0:T(8,128)(2,1)}, bf16[16,1]{0,1:T(2,128)(2,1)}), (bf16[16,1408]{1,0:T(8,128)(2,1)}, bf16[16,1408]{1,0:T(8,128)(2,1)}, bf16[16,1]{0,1:T(2,128)(2,1)})) %all-reduce.9.cloned.1.call-update) | async-done | bytes 90160 | tf_op jit(solution)/shard_map/psum | solution.py:37
  365.6 50.0 %all-reduce.13.cloned.1.call-done = (bf16[16,1408]{1,0:T(8,128)(2,1)}, bf16[16,1408]{1,0:T(8,128)(2,1)}, bf16[16,1]{0,1:T(2,128)(2,1)}) async-done(((bf16[16,1408]{1,0:T(8,128)(2,1)}, bf16[16,1408]{1,0:T(8,128)(2,1)}, bf16[16,1]{0,1:T(2,128)(2,1)}), (bf16[16,1408]{1,0:T(8,128)(2,1)}, bf16[16,1408]{1,0:T(8,128)(2,1)}, bf16[16,1]{0,1:T(2,128)(2,1)})) %all-reduce.13.cloned.1.call-update) | async-done | bytes 90160 | tf_op jit(solution)/shard_map/psum | solution.py:37
  415.6 0.6 rsqrt_bitcast_fusion
  416.2 1.0 fusion.36
  417.5 11.5 %all_to_all.55 = f32[8,1,256]{2,1,0:T(1,128)S(1)} all-to-all(f32[8,1,256]{2,1,0:T(1,128)S(1)} %reshape.1276), channel_id=1, replica_groups=mesh['kv_0'=8,'kv_1'=4,'tp'=8] {'tp'}, dimensions={0} | all-to-all | bytes 16384 | tf_op jit(solution)/shard_map/all_to_all | solution.py:48
  428.9 0.7 reduce.41
  429.7 0.6 add_convert_fusion
  (111 shorter events, 5.0 us)
Async XLA Ops:
  6.5 11.9 %copy-start = (bf16[128,1408]{1,0:T(8,128)(2,1)S(1)}, bf16[128,1408]{1,0:T(8,128)(2,1)}, u32[]{:S(2)}) copy-start(bf16[128,1408]{1,0:T(8,128)(2,1)} %param.22) | copy-start | bytes 1081348
  6.5 83.9 %all-reduce.11.cloned.1.call-start = ((), (), s32[]{:S(2)}) async-start(), calls=%async_computation.11 | async-start | bytes 181248 | tf_op jit(solution)/shard_map/psum | solution.py:37
  21.7 118.9 %all-reduce.15.cloned.1.call-start = ((), (), s32[]{:S(2)}) async-start(), calls=%async_computation.13 | async-start | bytes 181248 | tf_op jit(solution)/shard_map/psum | solution.py:37
  164.8 16.8 %all-to-all-start.4 = ((bf16[32,16,1]{1,2,0:T(2,128)(2,1)}), bf16[32,16,1]{1,2,0:T(2,128)(2,1)S(1)}, u32[]{:S(2)}, u32[]{:S(2)}) async-start(bf16[32,16,1]{1,2,0:T(2,128)(2,1)} %broadcast_in_dim.36), calls=%async_computation.4 | async-start | bytes 32768 | tf_op jit(solution)/shard_map/all_to_all | solution.py:22
  182.4 18.9 %all-to-all-start.3 = ((bf16[32,16,512]{2,1,0:T(8,128)(2,1)}), bf16[32,16,512]{2,1,0:T(8,128)(2,1)S(1)}, u32[]{:S(2)}, u32[]{:S(2)}) async-start(bf16[32,16,512]{2,1,0:T(8,128)(2,1)} %broadcast_in_dim.35), calls=%async_computation.3 | async-start | bytes 1048576 | tf_op jit(solution)/shard_map/all_to_all | solution.py:22
  186.3 7.5 %copy-start.5 = (bf16[512,128]{1,0:T(8,128)(2,1)S(1)}, bf16[512,128]{1,0:T(8,128)(2,1)}, u32[]{:S(2)}) copy-start(bf16[512,128]{1,0:T(8,128)(2,1)} %param.28) | copy-start | bytes 393220
  186.3 7.6 %copy-start.3 = (bf16[128,512]{1,0:T(8,128)(2,1)S(1)}, bf16[128,512]{1,0:T(8,128)(2,1)}, u32[]{:S(2)}) copy-start(bf16[128,512]{1,0:T(8,128)(2,1)} %param.26) | copy-start | bytes 393220
  186.3 22.1 %copy-start.9 = (s32[16]{0:T(128)S(1)}, s32[16]{0:T(128)}, u32[]{:S(2)}) copy-start(s32[16]{0:T(128)} %param.33) | copy-start | bytes 196
  186.3 22.2 %copy-start.4 = (bf16[128,512]{1,0:T(8,128)(2,1)S(1)}, bf16[128,512]{1,0:T(8,128)(2,1)}, u32[]{:S(2)}) copy-start(bf16[128,512]{1,0:T(8,128)(2,1)} %param.27) | copy-start | bytes 393220
  202.2 21.2 %all-to-all-start.5 = ((bf16[32,16,512]{2,1,0:T(8,128)(2,1)}), bf16[32,16,512]{2,1,0:T(8,128)(2,1)S(1)}, u32[]{:S(2)}, u32[]{:S(2)}) async-start(bf16[32,16,512]{2,1,0:T(8,128)(2,1)} %broadcast_in_dim.39), calls=%async_computation.5 | async-start | bytes 1048576 | tf_op jit(solution)/shard_map/all_to_all | solution.py:22
  224.2 46.7 %all-to-all-start.6 = ((bf16[32,16,512]{2,1,0:T(8,128)(2,1)}), bf16[32,16,512]{2,1,0:T(8,128)(2,1)S(1)}, u32[]{:S(2)}, u32[]{:S(2)}) async-start(bf16[32,16,512]{2,1,0:T(8,128)(2,1)} %broadcast_in_dim.40), calls=%async_computation.6 | async-start | bytes 1048576 | tf_op jit(solution)/shard_map/all_to_all | solution.py:22
  230.5 135.1 %all-reduce.9.cloned.1.call-start = ((), (), s32[]{:S(2)}) async-start(), calls=%async_computation.10 | async-start | bytes 181248 | tf_op jit(solution)/shard_map/psum | solution.py:37
  230.8 3.7 copy-start.10
  234.5 37.5 %copy-start.7 = (f32[4]{0:T(128)S(1)}, f32[4]{0:T(128)}, u32[]{:S(2)}) copy-start(f32[4]{0:T(128)} %param.29) | copy-start | bytes 52
  234.5 37.7 %copy-start.8 = (f32[128]{0:T(128)S(1)}, f32[128]{0:T(128)}, u32[]{:S(2)}) copy-start(f32[128]{0:T(128)} %param.30) | copy-start | bytes 1540
  234.6 64.6 %copy-start.1 = (bf16[128,1408]{1,0:T(8,128)(2,1)S(1)}, bf16[128,1408]{1,0:T(8,128)(2,1)}, u32[]{:S(2)}) copy-start(bf16[128,1408]{1,0:T(8,128)(2,1)} %param.36) | copy-start | bytes 1081348
  234.6 64.6 %copy-start.6 = (f32[128]{0:T(128)S(1)}, f32[128]{0:T(128)}, u32[]{:S(2)}) copy-start(f32[128]{0:T(128)} %param.34) | copy-start | bytes 1540
  234.6 65.4 %copy-start.2 = (bf16[128,1408]{1,0:T(8,128)(2,1)S(1)}, bf16[128,1408]{1,0:T(8,128)(2,1)}, u32[]{:S(2)}) copy-start(bf16[128,1408]{1,0:T(8,128)(2,1)} %param.35) | copy-start | bytes 1081348
  235.3 180.9 %copy-start.11 = (bf16[1408,128]{1,0:T(8,128)(2,1)S(1)}, bf16[1408,128]{1,0:T(8,128)(2,1)}, u32[]{:S(2)}) copy-start(bf16[1408,128]{1,0:T(8,128)(2,1)} %param.37) | copy-start | bytes 1081348
  300.8 114.8 %all-reduce.13.cloned.1.call-start = ((), (), s32[]{:S(2)}) async-start(), calls=%async_computation.12 | async-start | bytes 181248 | tf_op jit(solution)/shard_map/psum | solution.py:37
Sparse Core Ops, SparseCore 0:
  21.8 68.6 all-reduce.10
  92.9 47.5 all-reduce.14
  300.9 64.6 all-reduce.8
  367.9 47.5 all-reduce.12
where the time goes:
time: 438 us; the launch traced here: 437 us
  waiting for transfers between devices  262 us (60%)
  blocking collectives  97.2 us (22%)
  starting transfers between devices  24.7 us (6%)
  local copies, waits for them, and re-layouts  17.4 us (4%)
  between operations  13.7 us (3%)
  matrix products  12.4 us (3%)
  other arithmetic  9.27 us (2%)
    psum x4, waiting for transfers between devices, one_axis_at_a_time(): return functools.reduce(lax.psum, axes, array)  234 us
    all_to_all x3, blocking collectives, sent_and_summed(): lax.all_to_all(tiles, axis, split_axis=0, concat_axis=0, tiled=True)  40 us
    all_gather x2, blocking collectives, all_in_one(): both, at, found = (lax.all_gather(jnp.concatenate(lines), axis), 0, {})  31.7 us
    all_to_all x4, waiting for transfers between devices, sent_to_all(): return lax.all_to_all(copies, axis, split_axis=0, concat_axis=0, tiled=True)  28.7 us
    all_to_all x3, blocking collectives, sent_to_all(): return lax.all_to_all(copies, axis, split_axis=0, concat_axis=0, tiled=True)  25.5 us
    all_to_all x4, starting transfers between devices, sent_to_all(): return lax.all_to_all(copies, axis, split_axis=0, concat_axis=0, tiled=True)  24.5 us
  transfers between devices with their start and end apart: 8, of which 7 were waited for; matrix products, arithmetic and copies ran while one was open for 4% of the time, Pallas kernels for 0%

commit v1 on v0

v1 whole, which is shorter than its diff:
```python
import functools

import jax
import jax.numpy as jnp
from jax import lax
from jax.experimental import pallas as pl
from jax.experimental.pallas import tpu as pltpu
from jax.sharding import PartitionSpec as P

HEAD_DIM = 64
LANES = 128
MAPS = 2
EPSILON = 1e-06
NEG = -1e30
MESH = pl.DeviceIdType.MESH
F32 = jnp.float32
BF16 = jnp.bfloat16


def owner_of(b):
    return 4 * (b // 2) + 2 * (b % 2) + (b // 2) % 2


def split_in_two(value):
    high = value.astype(BF16).astype(F32)
    return high, value - high


def layer_kernel(
    dims,
    tokens,
    first_gain,
    mixer_gain,
    last_gain,
    head_gain,
    lam,
    lengths,
    first_gate,
    first_up,
    first_down,
    w_query,
    w_key,
    w_value,
    w_output,
    key_cache,
    value_cache,
    last_gate,
    last_up,
    last_down,
    result,
    v_gate1,
    v_up1,
    v_down1,
    v_query,
    v_key,
    v_value,
    v_output,
    v_keys,
    v_values,
    v_gate2,
    v_up2,
    v_down2,
    load_sem,
    tp_slots,
    tp_send,
    tp_recv,
    blocks,
    rows_f32,
    ffn_out,
    ffn_in,
    qkv_out,
    qkv_in,
    att_out,
    att_in,
    hid_all,
    query_all,
    head_all,
    own_rows,
    out_send,
    in_recv,
    all_send,
    all_recv,
):
    KV, TP, B, NH, FB, POS, WIDTH = dims
    FH = FB + 1
    k = lax.axis_index("kv")
    t = lax.axis_index("tp")
    is_owner = lax.rem(k, 2) == lax.rem(k // 4, 2)
    mine = k // 2

    loads = [
        (first_gate, v_gate1),
        (first_up, v_up1),
        (first_down, v_down1),
        (w_query, v_query),
        (w_key, v_key),
        (w_value, v_value),
        (key_cache, v_keys),
        (value_cache, v_values),
        (w_output, v_output),
        (last_gate, v_gate2),
        (last_up, v_up2),
        (last_down, v_down2),
    ]
    copies = [pltpu.make_async_copy(src, dst, load_sem.at[i]) for i, (src, dst) in enumerate(loads)]

    barrier = pltpu.get_barrier_semaphore()

    def greet_kv(d, _):
        pl.semaphore_signal(barrier, inc=1, device_id={"kv": lax.rem(k + d, KV)}, device_id_type=MESH)
        return 0

    def greet_tp(d, _):
        pl.semaphore_signal(barrier, inc=1, device_id={"tp": lax.rem(t + d, TP)}, device_id_type=MESH)
        return 0

    lax.fori_loop(1, KV, greet_kv, 0)
    lax.fori_loop(1, TP, greet_tp, 0)
    for copy in copies:
        copy.start()
    pl.semaphore_wait(barrier, KV - 1 + TP - 1)

    def tp_copy(turn, d):
        return pltpu.make_async_remote_copy(
            src_ref=tp_slots.at[turn, t],
            dst_ref=tp_slots.at[turn, t],
            send_sem=tp_send.at[turn, d],
            recv_sem=tp_recv.at[turn, d],
            device_id={"tp": lax.rem(t + d, TP)},
            device_id_type=MESH,
        )

    def tp_sum(turn, value):
        tp_slots[turn, t] = value

        def send(d, _):
            tp_copy(turn, d).start()
            return 0

        def take(d, _):
            tp_copy(turn, d).wait()
            return 0

        lax.fori_loop(1, TP, send, 0)
        lax.fori_loop(1, TP, take, 0)
        total = tp_slots[turn, 0]
        for s in range(1, TP):
            total = total + tp_slots[turn, s]
        return total

    def out_copy(turn, b, source, out_ref, in_ref):
        return pltpu.make_async_remote_copy(
            src_ref=out_ref.at[b],
            dst_ref=in_ref.at[source],
            send_sem=out_send.at[turn, b],
            recv_sem=in_recv.at[turn, source],
            device_id={"kv": owner_of(b)},
            device_id_type=MESH,
        )

    def send_row(turn, b, out_ref, in_ref):
        there = owner_of(b)

        @pl.when(there != k)
        def _():
            out_copy(turn, b, k, out_ref, in_ref).start()

        @pl.when(there == k)
        def _():
            in_ref[k] = out_ref[b]

    def send_rows(turn, out_ref, in_ref):
        def send(i, _):
            send_row(turn, lax.rem(mine + B // 2 + i, B), out_ref, in_ref)
            return 0

        lax.fori_loop(0, B, send, 0)

    def take_rows(turn, out_ref, in_ref):
        def take(d, _):
            out_copy(turn, mine, lax.rem(k + d, KV), out_ref, in_ref).wait_recv()
            return 0

        lax.fori_loop(1, KV, take, 0)

    def all_copy(turn, b, d, ref):
        return pltpu.make_async_remote_copy(
            src_ref=ref.at[b],
            dst_ref=ref.at[b],
            send_sem=all_send.at[turn, d],
            recv_sem=all_recv.at[turn, b],
            device_id={"kv": lax.rem(k + d, KV)},
            device_id_type=MESH,
        )

    def share_row(turn, ref):
        def send(i, _):
            d = 1 + lax.rem(i + KV // 2 - 1, KV - 1)
            all_copy(turn, mine, d, ref).start()
            return 0

        lax.fori_loop(0, KV - 1, send, 0)

    def take_all(turn, ref):
        def take(b, _):
            @pl.when(owner_of(b) != k)
            def _():
                all_copy(turn, b, 1, ref).wait_recv()

            return 0

        lax.fori_loop(0, B, take, 0)

    def as_lhs(ref, count):
        rows = ref.shape[1]
        rows_f32[0 : B * rows, :] = ref[...].astype(F32).reshape(B * rows, LANES)
        parts = [rows_f32[pl.ds(c, B, stride=rows), :] for c in range(count)]
        return jnp.concatenate(parts, axis=1).astype(BF16)

    def put_block(c, value):
        blocks[c * B : (c + 1) * B, :] = value

    def pack_rows(count, out_ref):
        for b in range(B):
            out_ref[b] = blocks[pl.ds(b, count, stride=B), :].astype(BF16)

    def normed_rows(stream, gain):
        squares = jnp.sum(stream * stream, axis=1, keepdims=True)
        high, low = split_in_two(jnp.broadcast_to(squares, (B, LANES)))
        return (stream * gain[...]).astype(BF16), high, low

    def gated_units(turn, stream, gain, gate_w, up_w, down_w, waits):
        scaled, high, low = normed_rows(stream, gain)
        put_block(FB, high)
        put_block(FH + FB, low)
        for at, weight, wait in ((0, gate_w, waits[0]), (FH, up_w, waits[1])):
            wait.wait()
            part = jnp.dot(scaled, weight[...], preferred_element_type=F32)
            for c in range(FB):
                put_block(at + c, part[:, c * LANES : (c + 1) * LANES])
        out_ref, in_ref = ffn_out.at[turn], ffn_in.at[turn]
        hid_ref = hid_all.at[turn]
        pack_rows(2 * FH, out_ref)
        send_rows(3 * turn, out_ref, in_ref)

        @pl.when(is_owner)
        def _():
            take_rows(3 * turn, out_ref, in_ref)
            total = jnp.sum(in_ref[...].astype(F32), axis=0)
            squares = total[FB : FB + 1] + total[FH + FB : FH + FB + 1]
            inv = lax.rsqrt(squares / WIDTH + EPSILON)
            gate = total[0:FH] * inv
            up = total[FH : 2 * FH] * inv
            hid = jax.nn.silu(gate) * up
            hid = jnp.where(lax.broadcasted_iota(jnp.int32, hid.shape, 0) < FB, hid, 0.0)
            pad = hid_ref.shape[1] - FH
            hid_ref[mine] = jnp.concatenate([hid, jnp.zeros((pad, LANES), F32)], axis=0).astype(BF16)
            share_row(3 * turn, hid_ref)

        take_all(3 * turn, hid_ref)
        hidden = as_lhs(hid_ref, FB)
        waits[2].wait()
        return jnp.dot(hidden, down_w[...], preferred_element_type=F32)

    tokens_f32 = tokens[...].astype(F32)
    columns = tokens_f32.shape[1]
    wide = jnp.concatenate([tokens_f32, jnp.zeros((B, LANES - columns), F32)], axis=1)
    stream = tp_sum(0, pltpu.roll(wide, t * columns, 1))

    part = gated_units(0, stream, first_gain, v_gate1, v_up1, v_down1, copies[0:3])
    first = (stream + 0.5 * tp_sum(1, part)).astype(BF16).astype(F32)

    scaled, high, low = normed_rows(first, mixer_gain)
    for n, weight in enumerate((v_query, v_key, v_value)):
        copies[3 + n].wait()
        part = jnp.dot(scaled, weight[...], preferred_element_type=F32)
        for c in range(NH):
            put_block(NH * n + c, part[:, c * LANES : (c + 1) * LANES])
    put_block(3 * NH, high)
    put_block(3 * NH + 1, low)
    put_block(3 * NH + 2, jnp.zeros((B, LANES), F32))
    put_block(3 * NH + 3, jnp.zeros((B, LANES), F32))
    pack_rows(4 * NH, qkv_out)
    send_rows(1, qkv_out, qkv_in)

    @pl.when(is_owner)
    def _():
        take_rows(1, qkv_out, qkv_in)
        total = jnp.sum(qkv_in[...].astype(F32), axis=0)
        squares = total[3 * NH : 3 * NH + 1] + total[3 * NH + 1 : 3 * NH + 2]
        inv = lax.rsqrt(squares / WIDTH + EPSILON)
        rows = (total[0 : 3 * NH] * inv).astype(BF16).astype(F32)
        query, new_key, new_value = rows[0:NH], rows[NH : 2 * NH], rows[2 * NH : 3 * NH]
        first_map = lax.broadcasted_iota(jnp.int32, (NH, LANES), 1) < HEAD_DIM
        query = query * HEAD_DIM ** (-0.5)
        both = jnp.concatenate(
            [jnp.where(first_map, query, 0.0), jnp.where(first_map, 0.0, query)], axis=0
        )
        query_all[mine] = both.astype(BF16)
        share_row(1, query_all)
        own = jnp.sum(both * jnp.concatenate([new_key, new_key], axis=0), axis=1, keepdims=True)
        own_rows[0] = jnp.broadcast_to(own, (MAPS * NH, LANES))
        own_rows[1] = jnp.concatenate([new_value, new_value], axis=0)

    take_all(1, query_all)

    copies[6].wait()
    copies[7].wait()
    span = POS * NH
    row = lax.broadcasted_iota(jnp.int32, (MAPS * NH, span), 0)
    lane = lax.broadcasted_iota(jnp.int32, (MAPS * NH, span), 1)
    own_head = lax.rem(lane, NH) == lax.rem(row, NH)
    position = k * POS + lane // NH
    stat_lane = lax.broadcasted_iota(jnp.int32, (MAPS * NH, LANES), 1)

    def attend(i, _):
        b = lax.rem(mine + B // 2 + i, B)
        scores = lax.dot_general(
            query_all[b], v_keys[b], (((1,), (1,)), ((), ())), preferred_element_type=F32
        )
        live = jnp.logical_and(own_head, position < lengths[b])
        scores = jnp.where(live, scores, NEG)
        peak_high, peak_low = split_in_two(jnp.max(scores, axis=1, keepdims=True))
        peak_low = peak_low.astype(BF16).astype(F32)
        weights = jnp.where(live, jnp.exp(scores - (peak_high + peak_low)), 0.0)
        den_high, den_low = split_in_two(jnp.sum(weights, axis=1, keepdims=True))
        num = jnp.dot(weights.astype(BF16), v_values[b], preferred_element_type=F32)
        stats = jnp.where(
            stat_lane < 64,
            jnp.where(stat_lane < 32, peak_high, peak_low),
            jnp.where(stat_lane < 96, den_high, den_low),
        )
        att_out[b] = jnp.concatenate([num, stats], axis=0).astype(BF16)
        send_row(2, b, att_out, att_in)
        return 0

    lax.fori_loop(0, B, attend, 0)

    @pl.when(is_owner)
    def _():
        take_rows(2, att_out, att_in)
        arrived = att_in[...].astype(F32)
        num, stats = arrived[:, 0 : MAPS * NH], arrived[:, MAPS * NH : 2 * MAPS * NH]
        peak = stats[:, :, 0:1] + stats[:, :, 32:33]
        den = stats[:, :, 64:65] + stats[:, :, 96:97]
        own = own_rows[0][:, 0:1]
        highest = jnp.maximum(jnp.max(peak, axis=0), own)
        scale = jnp.exp(peak - highest[None])
        own_weight = jnp.exp(own - highest)
        own_round = own_weight.astype(BF16).astype(F32)
        total = jnp.sum(scale * den, axis=0) + own_weight
        weighted = jnp.sum(scale * num, axis=0) + own_round * own_rows[1]
        mixed = weighted / total
        head = lax.broadcasted_iota(jnp.int32, (NH, 1), 0)
        lam_rows = jnp.zeros((NH, 1), F32)
        for h in range(NH):
            lam_rows = jnp.where(head == h, lam[h], lam_rows)
        mixed = mixed[0:NH] - lam_rows * mixed[NH : 2 * NH]
        inv = lax.rsqrt(jnp.mean(mixed * mixed, axis=1, keepdims=True) + EPSILON)
        normed = mixed * inv * head_gain[...]
        head_all[mine] = jnp.concatenate([normed, jnp.zeros((NH, LANES), F32)], axis=0).astype(BF16)
        share_row(2, head_all)

    take_all(2, head_all)
    attended = as_lhs(head_all, NH)
    copies[8].wait()
    part = jnp.dot(attended, v_output[...], preferred_element_type=F32)
    second = (first + tp_sum(2, part)).astype(BF16).astype(F32)

    part = gated_units(1, second, last_gain, v_gate2, v_up2, v_down2, copies[9:12])
    last = second + 0.5 * tp_sum(3, part)
    own_columns = lax.rem(LANES - t * columns, LANES)
    result[...] = pltpu.roll(last, own_columns, 1)[:, 0:columns].astype(BF16)

    def sent_rows(turn, out_ref, in_ref):
        def sent(b, _):
            @pl.when(owner_of(b) != k)
            def _():
                out_copy(turn, b, k, out_ref, in_ref).wait_send()

            return 0

        lax.fori_loop(0, B, sent, 0)

    def sent_all(turn, ref):
        @pl.when(is_owner)
        def _():
            def sent(d, _):
                all_copy(turn, mine, d, ref).wait_send()
                return 0

            lax.fori_loop(1, KV, sent, 0)

    sent_rows(0, ffn_out.at[0], ffn_in.at[0])
    sent_rows(1, qkv_out, qkv_in)
    sent_rows(2, att_out, att_in)
    sent_rows(3, ffn_out.at[1], ffn_in.at[1])
    sent_all(0, hid_all.at[0])
    sent_all(1, query_all)
    sent_all(2, head_all)
    sent_all(3, hid_all.at[1])


def on_device(KV, TP):
    def run(
        tokens,
        first_gain,
        first_gate,
        first_up,
        first_down,
        mixer_gain,
        w_query,
        w_key,
        w_value,
        w_output,
        lam_heads,
        head_gain,
        key_cache,
        value_cache,
        lengths,
        last_gain,
        last_gate,
        last_up,
        last_down,
    ):
        B, POS, NH, _ = key_cache.shape
        FB = first_gate.shape[1] // LANES
        FH = FB + 1
        HR = -(-FH // 8) * 8
        WIDTH = w_query.shape[0] * KV
        dims = (KV, TP, B, NH, FB, POS, WIDTH)
        vmem = pl.BlockSpec(memory_space=pltpu.VMEM)
        smem = pl.BlockSpec(memory_space=pltpu.SMEM)
        far = pl.BlockSpec(memory_space=pl.ANY)
        flat_keys = key_cache.reshape(B, POS * NH, LANES)
        flat_values = value_cache.reshape(B, POS * NH, LANES)
        large = (first_gate, first_up, first_down, w_query, w_key, w_value, w_output)
        large += (flat_keys, flat_values, last_gate, last_up, last_down)
        return pl.pallas_call(
            functools.partial(layer_kernel, dims),
            out_shape=jax.ShapeDtypeStruct(tokens.shape, BF16),
            in_specs=[vmem] * 5 + [smem] * 2 + [far] * 12,
            out_specs=vmem,
            scratch_shapes=[
                *(pltpu.VMEM(a.shape, a.dtype) for a in large),
                pltpu.SemaphoreType.DMA((12,)),
                pltpu.VMEM((4, TP, B, LANES), F32),
                pltpu.SemaphoreType.DMA((4, TP)),
                pltpu.SemaphoreType.DMA((4, TP)),
                pltpu.VMEM((max(2 * FH, 4 * NH) * B, LANES), F32),
                pltpu.VMEM((max(HR, 2 * NH) * B, LANES), F32),
                pltpu.VMEM((2, B, 2 * FH, LANES), BF16),
                pltpu.VMEM((2, KV, 2 * FH, LANES), BF16),
                pltpu.VMEM((B, 4 * NH, LANES), BF16),
                pltpu.VMEM((KV, 4 * NH, LANES), BF16),
                pltpu.VMEM((B, 4 * NH, LANES), BF16),
                pltpu.VMEM((KV, 4 * NH, LANES), BF16),
                pltpu.VMEM((2, B, HR, LANES), BF16),
                pltpu.VMEM((B, 2 * NH, LANES), BF16),
                pltpu.VMEM((B, 2 * NH, LANES), BF16),
                pltpu.VMEM((2, 2 * NH, LANES), F32),
                pltpu.SemaphoreType.DMA((4, B)),
                pltpu.SemaphoreType.DMA((4, KV)),
                pltpu.SemaphoreType.DMA((4, KV)),
                pltpu.SemaphoreType.DMA((4, B)),
            ],
            compiler_params=pltpu.CompilerParams(collective_id=0, has_side_effects=True),
        )(
            tokens,
            first_gain.reshape(1, LANES),
            mixer_gain.reshape(1, LANES),
            last_gain.reshape(1, LANES),
            head_gain.reshape(1, LANES),
            lam_heads,
            lengths,
            first_gate,
            first_up,
            first_down,
            w_query,
            w_key,
            w_value,
            w_output,
            flat_keys,
            flat_values,
            last_gate,
            last_up,
            last_down,
        )

    return run


def solution(mesh):
    return jax.shard_map(
        on_device(mesh.shape["kv"], mesh.shape["tp"]),
        mesh=mesh,
        in_specs=(
            P(None, ("kv", "tp")),
            P("kv"),
            P("kv", "tp"),
            P("kv", "tp"),
            P("tp", "kv"),
            P("kv"),
            P("kv", "tp"),
            P("kv", "tp"),
            P("kv", "tp"),
            P("tp", "kv"),
            P("tp"),
            P(),
            P(None, "kv", "tp", None),
            P(None, "kv", "tp", None),
            P(),
            P("kv"),
            P("kv", "tp"),
            P("kv", "tp"),
            P("tp", "kv"),
        ),
        out_specs=P(None, ("kv", "tp")),
        check_vma=False,
    )
```

time: 438 us -> 95 us (0.22)
  waiting for transfers between devices: 262 us -> 0 us
  blocking collectives: 97.2 us -> 0 us
  Pallas kernels: 0 us -> 93.6 us
  starting transfers between devices: 24.7 us -> 0 us
  local copies, waits for them, and re-layouts: 17.4 us -> 1.28 us
  between operations: 13.7 us -> 0.01 us
  matrix products: 12.4 us -> 0 us
  other arithmetic: 9.27 us -> 0 us
    psum x4 -> x0, waiting for transfers between devices: 234 us -> none  [one_axis_at_a_time(): return functools.reduce(lax.psum, axes, array)]
    pallas_call x0 -> x1, Pallas kernels: none -> 93.6 us  [run(): pl.pallas_call(functools.partial(layer_kernel, dims), out_shape=jax.Shape...]
    all_to_all x6 -> x0, blocking collectives: 65.5 us -> none  [the longest x3 40 us: sent_and_summed(): lax.all_to_all(tiles, axis, split_axis=0, concat_axis=0, tiled=True)]
    all_gather x2 -> x0, blocking collectives: 31.7 us -> none  [all_in_one(): both, at, found = (lax.all_gather(jnp.concatenate(lines), axis), 0, {})]
    all_to_all x4 -> x0, waiting for transfers between devices: 28.7 us -> none  [sent_to_all(): return lax.all_to_all(copies, axis, split_axis=0, concat_axis=0, tiled=True)]
    all_to_all x4 -> x0, starting transfers between devices: 24.5 us -> none  [sent_to_all(): return lax.all_to_all(copies, axis, split_axis=0, concat_axis=0, tiled=True)]
    dot_general x12 -> x0, matrix products: 12.4 us -> none  [the longest x1 3 us: attend(): jnp.einsum('bhmd,bphmd->bhmp', query_rows, key_entries, preferred_element...]
    unnamed x38 -> x1, local copies, waits for them, and re-layouts: 8.64 us -> 1.28 us
  transfers between devices with their start and end apart: 8 -> 0, of which waited for: 7 -> 0; matrix products, arithmetic and copies ran while one was open for 4% -> 0% of each run, Pallas kernels for 0% -> 0%
where the time goes in v1:
time: 95 us; the launch traced here: 94.8 us
  Pallas kernels  93.6 us (99%)
  local copies, waits for them, and re-layouts  1.28 us (1%)
    pallas_call x1, Pallas kernels, run(): pl.pallas_call(functools.partial(layer_kernel, dims), out_shape=jax.Shape...  93.6 us

profile of v1, /device:TPU:1, one launch (start us, length us, event | category | flops | bytes accessed | tf_op | source)
XLA Modules:
  0.0 94.8 jit_solution(5852921679797153616)
XLA Ops:
  0.0 93.6 %shard_map.181 = bf16[16,16]{1,0:T(8,128)(2,1)} custom-call(bf16[16,16]{1,0:T(8,128)(2,1)} %tokens.1, f32[1,128]{1,0:T(1,128)} %bitcast.8, f32[1,128]{1,0:T(1,128)} %bitcast.9, f32[1,128]{1,0:T(1,128)} %bitcast.10, f32[1,128]{1,0:T(1,128)} %bitcast.11, f32[4]{0:T(128)} %lam.1, s32[16]{0:T(128)} %lengths.1, bf16[128,1408]{1,0:T(8,128)(2,1)} %first_gate.1, ...), custom_call_target="tpu_custom_call" | custom-call | tf_op jit(solution)/shard_map/pallas_call | solution.py:439
  93.6 1.3 %copy.21 = bf16[16,16]{1,0:T(8,128)(2,1)} copy(bf16[16,16]{1,0:T(8,128)(2,1)} %shard_map.181) | data formatting | bytes 1024

commit v2 on v1

v2 whole, which is shorter than its diff:
```python
import functools

import jax
import jax.numpy as jnp
from jax import lax
from jax.experimental import pallas as pl
from jax.experimental.pallas import tpu as pltpu
from jax.sharding import PartitionSpec as P

HEAD_DIM = 64
LANES = 128
MAPS = 2
EPSILON = 1e-06
NEG = -(2.0**100)
MESH = pl.DeviceIdType.MESH
F32 = jnp.float32
BF16 = jnp.bfloat16


def server_of(b, t):
    z = b // 2
    return 4 * z + 2 * lax.rem(b, 2) + lax.rem(z + 1 + t, 2), t + 1 - lax.rem(t, 2)


def split_in_two(value):
    high = value.astype(BF16).astype(F32)
    return high, value - high


def layer_kernel(
    dims,
    tokens,
    first_gain,
    mixer_gain,
    last_gain,
    head_gain,
    lam,
    lengths,
    first_gate,
    first_up,
    first_down,
    w_query,
    w_key,
    w_value,
    w_output,
    key_cache,
    value_cache,
    last_gate,
    last_up,
    last_down,
    result,
    v_gate1,
    v_up1,
    v_down1,
    v_query,
    v_key,
    v_value,
    v_output,
    v_keys,
    v_values,
    v_gate2,
    v_up2,
    v_down2,
    v_tokens,
    v_gain1,
    v_gain2,
    v_gain3,
    v_head_gain,
    load_sem,
    tp_slots,
    tp_send,
    tp_recv,
    blocks,
    rows_f32,
    ffn_out,
    ffn_in,
    qkv_out,
    qkv_in,
    att_out,
    att_in,
    hid_row,
    hid_all,
    query_row,
    query_all,
    head_row,
    head_all,
    own_rows,
    long_rows,
    short_rows,
    out_send,
    in_recv,
    all_send,
    all_recv,
):
    KV, TP, B, NH, FB, POS, WIDTH = dims
    FH = FB + 1
    Y, Z = 4, KV // 4
    k = lax.axis_index("kv")
    t = lax.axis_index("tp")
    mine = k // 2
    serves = lax.rem(t, 2) == 1
    group = t - lax.rem(k + k // 4, 2)
    home = jnp.logical_and(serves, group == t)
    away = jnp.logical_and(serves, group != t)

    loads = [
        (first_gate, v_gate1),
        (first_up, v_up1),
        (first_down, v_down1),
        (w_query, v_query),
        (w_key, v_key),
        (w_value, v_value),
        (key_cache, v_keys),
        (value_cache, v_values),
        (w_output, v_output),
        (last_gate, v_gate2),
        (last_up, v_up2),
        (last_down, v_down2),
        (tokens, v_tokens),
        (first_gain, v_gain1),
        (mixer_gain, v_gain2),
        (last_gain, v_gain3),
        (head_gain, v_head_gain),
    ]
    copies = [pltpu.make_async_copy(src, dst, load_sem.at[i]) for i, (src, dst) in enumerate(loads)]

    def from_far(i, size):
        half = (i + 1) // 2
        return lax.rem(size // 2 + half * (1 - 2 * lax.rem(i, 2)), size)

    def kv_from_far(i):
        z = lax.rem(k // Y + from_far(i // Y, Z), Z)
        y = lax.rem(lax.rem(k, Y) + from_far(lax.rem(i, Y), Y), Y)
        return z * Y + y

    def row_from_far(i):
        z = lax.rem(k // Y + from_far(i // 2, Z), Z)
        return 2 * z + lax.rem(mine + 1 + i, 2)

    barrier = pltpu.get_barrier_semaphore()

    def greet(kv, tp):
        pl.semaphore_signal(barrier, inc=1, device_id={"kv": kv, "tp": tp}, device_id_type=MESH)

    def greet_server(i, _):
        b = row_from_far(i)

        @pl.when(jnp.logical_not(jnp.logical_and(home, b == mine)))
        def _():
            greet(*server_of(b, t))

        return 0

    def greet_group(i, _):
        there = kv_from_far(i)

        @pl.when(jnp.logical_not(jnp.logical_and(home, there == k)))
        def _():
            greet(there, group)

        return 0

    def greet_tp(d, _):
        greet(k, lax.rem(t + d, TP))
        return 0

    with jax.named_scope("greet"):

        @pl.when(serves)
        def _():
            lax.fori_loop(0, KV, greet_group, 0)

        lax.fori_loop(0, B, greet_server, 0)
        lax.fori_loop(1, TP, greet_tp, 0)
    for copy in copies[12:] + copies[:12]:
        copy.start()
    for copy in copies[12:]:
        copy.wait()

    with jax.named_scope("barrier"):

        @pl.when(home)
        def _():
            pl.semaphore_wait(barrier, B - 1 + KV - 1 + TP - 1)

        @pl.when(away)
        def _():
            pl.semaphore_wait(barrier, B + KV + TP - 1)

        @pl.when(jnp.logical_not(serves))
        def _():
            pl.semaphore_wait(barrier, B + TP - 1)

    def remote(src, dst, send_sem, recv_sem, kv, tp):
        return pltpu.make_async_remote_copy(
            src_ref=src,
            dst_ref=dst,
            send_sem=send_sem,
            recv_sem=recv_sem,
            device_id={"kv": kv, "tp": tp},
            device_id_type=MESH,
        )

    def all_of(ref, count, send_sem, recv_sem):
        some = ref.at[pl.ds(0, count)]
        return remote(some, some, send_sem, recv_sem, k, t)

    def tp_sum(turn, value):
        slot = tp_slots.at[turn, t]
        slot[...] = value.astype(BF16)
        send_sem, recv_sem = tp_send.at[turn], tp_recv.at[turn]

        def send(d, _):
            remote(slot, slot, send_sem, recv_sem, k, lax.rem(t + d, TP)).start()
            return 0

        with jax.named_scope(f"tp_send{turn}"):
            lax.fori_loop(1, TP, send, 0, unroll=True)
        with jax.named_scope(f"tp_take{turn}"):
            arrived = all_of(tp_slots.at[turn], TP - 1, send_sem, recv_sem)
            arrived.wait_send()
            arrived.wait_recv()
        return jnp.sum(tp_slots[turn].astype(F32), axis=0)

    def send_row(turn, b, out_ref, in_ref):
        here = jnp.logical_and(home, b == mine)

        @pl.when(jnp.logical_not(here))
        def _():
            kv, tp = server_of(b, t)
            remote(out_ref.at[b], in_ref.at[k], out_send.at[turn], in_recv.at[turn], kv, tp).start()

        @pl.when(here)
        def _():
            in_ref[k] = out_ref[b]

    def send_rows(turn, out_ref, in_ref):
        def send(i, _):
            send_row(turn, row_from_far(i), out_ref, in_ref)
            return 0

        with jax.named_scope(f"rows_send{turn}"):
            lax.fori_loop(0, B, send, 0)

    def take_rows(turn, out_ref, in_ref):
        with jax.named_scope(f"rows_take{turn}"):

            @pl.when(home)
            def _():
                all_of(in_ref, KV - 1, out_send.at[turn], in_recv.at[turn]).wait_recv()

            @pl.when(away)
            def _():
                all_of(in_ref, KV, out_send.at[turn], in_recv.at[turn]).wait_recv()

    def share_row(turn, row_ref, all_ref):
        def send(i, _):
            there = kv_from_far(i)

            @pl.when(jnp.logical_not(jnp.logical_and(home, there == k)))
            def _():
                remote(row_ref, all_ref.at[mine], all_send.at[turn], all_recv.at[turn], there, group).start()

            return 0

        with jax.named_scope(f"all_send{turn}"):
            lax.fori_loop(0, KV, send, 0)

            @pl.when(home)
            def _():
                all_ref[mine] = row_ref[...]

    def take_all(turn, out_ref, rows_ref, all_ref):
        with jax.named_scope(f"all_take{turn}"):

            @pl.when(home)
            def _():
                all_of(out_ref, B - 1, out_send.at[turn], in_recv.at[turn]).wait_send()
                all_of(rows_ref, KV - 1, all_send.at[turn], all_recv.at[turn]).wait_send()
                all_of(all_ref, B - 1, all_send.at[turn], all_recv.at[turn]).wait_recv()

            @pl.when(away)
            def _():
                all_of(rows_ref, KV, all_send.at[turn], all_recv.at[turn]).wait_send()

            @pl.when(jnp.logical_not(home))
            def _():
                all_of(out_ref, B, out_send.at[turn], in_recv.at[turn]).wait_send()
                all_of(all_ref, B, all_send.at[turn], all_recv.at[turn]).wait_recv()

    def as_lhs(ref, count):
        rows = ref.shape[1]
        rows_f32[0 : B * rows, :] = ref[...].astype(F32).reshape(B * rows, LANES)
        parts = [rows_f32[pl.ds(c, B, stride=rows), :] for c in range(count)]
        return jnp.concatenate(parts, axis=1).astype(BF16)

    def put_block(c, value):
        blocks[c * B : (c + 1) * B, :] = value

    def pack_rows(count, out_ref):
        for b in range(B):
            out_ref[b] = blocks[pl.ds(b, count, stride=B), :].astype(BF16)

    def normed_rows(stream, gain):
        squares = jnp.sum(stream * stream, axis=1, keepdims=True)
        high, low = split_in_two(jnp.broadcast_to(squares, (B, LANES)))
        return (stream * gain[...]).astype(BF16), high, low

    def gated_units(turn, stream, gain, gate_w, up_w, down_w, waits):
        scaled, high, low = normed_rows(stream, gain)
        put_block(FB, high)
        put_block(FH + FB, low)
        for at, weight, wait in ((0, gate_w, waits[0]), (FH, up_w, waits[1])):
            wait.wait()
            part = jnp.dot(scaled, weight[...], preferred_element_type=F32)
            for c in range(FB):
                put_block(at + c, part[:, c * LANES : (c + 1) * LANES])
        out_ref, in_ref = ffn_out.at[turn], ffn_in.at[turn]
        row_ref, all_ref = hid_row.at[turn], hid_all.at[turn]
        with jax.named_scope("pack"):
            pack_rows(2 * FH, out_ref)
        send_rows(3 * turn, out_ref, in_ref)

        @pl.when(serves)
        def _():
            take_rows(3 * turn, out_ref, in_ref)
            total = jnp.sum(in_ref[...].astype(F32), axis=0)
            squares = total[FB : FB + 1] + total[FH + FB : FH + FB + 1]
            inv = lax.rsqrt(squares / WIDTH + EPSILON)
            gate = total[0:FH] * inv
            up = total[FH : 2 * FH] * inv
            hid = jax.nn.silu(gate) * up
            hid = jnp.where(lax.broadcasted_iota(jnp.int32, hid.shape, 0) < FB, hid, 0.0)
            pad = row_ref.shape[0] - FH
            row_ref[...] = jnp.concatenate([hid, jnp.zeros((pad, LANES), F32)], axis=0).astype(BF16)
            share_row(3 * turn, row_ref, all_ref)

        take_all(3 * turn, out_ref, long_rows, all_ref)
        with jax.named_scope("lhs"):
            hidden = as_lhs(all_ref, FB)
        waits[2].wait()
        return jnp.dot(hidden, down_w[...], preferred_element_type=F32)

    tokens_f32 = v_tokens[...].astype(F32)
    columns = tokens_f32.shape[1]
    wide = jnp.concatenate([tokens_f32, jnp.zeros((B, LANES - columns), F32)], axis=1)
    stream = tp_sum(0, pltpu.roll(wide, t * columns, 1))

    part = gated_units(0, stream, v_gain1, v_gate1, v_up1, v_down1, copies[0:3])
    first = (stream + 0.5 * tp_sum(1, part)).astype(BF16).astype(F32)

    scaled, high, low = normed_rows(first, v_gain2)
    for n, weight in enumerate((v_query, v_key, v_value)):
        copies[3 + n].wait()
        part = jnp.dot(scaled, weight[...], preferred_element_type=F32)
        for c in range(NH):
            put_block(NH * n + c, part[:, c * LANES : (c + 1) * LANES])
    put_block(3 * NH, high)
    put_block(3 * NH + 1, low)
    section = lax.broadcasted_iota(jnp.int32, (B, LANES), 1) // (LANES // NH)
    lam_row = jnp.zeros((B, LANES), F32)
    for h in range(NH):
        lam_row = jnp.where(section == h, lam[h], lam_row)
    high, low = split_in_two(jnp.where(k == 0, lam_row, 0.0))
    put_block(3 * NH + 2, high)
    put_block(3 * NH + 3, low)
    pack_rows(4 * NH, qkv_out)
    send_rows(1, qkv_out, qkv_in)

    @pl.when(serves)
    def _():
        take_rows(1, qkv_out, qkv_in)
        total = jnp.sum(qkv_in[...].astype(F32), axis=0)
        squares = total[3 * NH : 3 * NH + 1] + total[3 * NH + 1 : 3 * NH + 2]
        inv = lax.rsqrt(squares / WIDTH + EPSILON)
        rows = (total[0 : 3 * NH] * inv).astype(BF16).astype(F32)
        query, new_key, new_value = rows[0:NH], rows[NH : 2 * NH], rows[2 * NH : 3 * NH]
        first_map = lax.broadcasted_iota(jnp.int32, (NH, LANES), 1) < HEAD_DIM
        query = query * HEAD_DIM ** (-0.5)
        both = jnp.concatenate(
            [jnp.where(first_map, query, 0.0), jnp.where(first_map, 0.0, query)], axis=0
        )
        query_row[...] = both.astype(BF16)
        share_row(1, query_row, query_all)
        own = jnp.sum(both * jnp.concatenate([new_key, new_key], axis=0), axis=1, keepdims=True)
        own_rows[0] = jnp.broadcast_to(own, (MAPS * NH, LANES))
        own_rows[1] = jnp.concatenate([new_value, new_value], axis=0)
        lam_sum = total[3 * NH + 2 : 3 * NH + 3] + total[3 * NH + 3 : 3 * NH + 4]
        own_rows[2] = jnp.broadcast_to(lam_sum, (MAPS * NH, LANES))

    take_all(1, qkv_out, short_rows, query_all)

    copies[6].wait()
    copies[7].wait()
    span = POS * NH
    row = lax.broadcasted_iota(jnp.int32, (MAPS * NH, span), 0)
    lane = lax.broadcasted_iota(jnp.int32, (MAPS * NH, span), 1)
    own_head = lax.rem(lane, NH) == lax.rem(row, NH)
    position = jnp.where(own_head, k * POS + lane // NH, KV * POS)
    stat_lane = lax.broadcasted_iota(jnp.int32, (MAPS * NH, LANES), 1)
    SIDE = 4

    def attend(i, _):
        rows_b = [row_from_far(i * SIDE + j) for j in range(SIDE)]
        scores = [
            lax.dot_general(
                query_all[b], v_keys[b], (((1,), (1,)), ((), ())), preferred_element_type=F32
            )
            for b in rows_b
        ]
        scores = [jnp.where(position < lengths[b], s, NEG) for b, s in zip(rows_b, scores)]
        peaks = [split_in_two(jnp.max(s, axis=1, keepdims=True)) for s in scores]
        peaks = [(high, low.astype(BF16).astype(F32)) for high, low in peaks]
        weights = [jnp.exp(s - (high + low)) for s, (high, low) in zip(scores, peaks)]
        nums = [
            jnp.dot(w.astype(BF16), v_values[b], preferred_element_type=F32)
            for b, w in zip(rows_b, weights)
        ]
        for b, w, num, (high, low) in zip(rows_b, weights, nums, peaks):
            den_high, den_low = split_in_two(jnp.sum(w, axis=1, keepdims=True))
            stats = jnp.where(
                stat_lane < 64,
                jnp.where(stat_lane < 32, high, low),
                jnp.where(stat_lane < 96, den_high, den_low),
            )
            att_out[b] = jnp.concatenate([num, stats], axis=0).astype(BF16)
        for b in rows_b:
            send_row(2, b, att_out, att_in)
        return 0

    with jax.named_scope("attend"):
        lax.fori_loop(0, B // SIDE, attend, 0)

    @pl.when(serves)
    def _():
        take_rows(2, att_out, att_in)
        arrived = att_in[...].astype(F32)
        num, stats = arrived[:, 0 : MAPS * NH], arrived[:, MAPS * NH : 2 * MAPS * NH]
        peak = stats[:, :, 0:1] + stats[:, :, 32:33]
        den = stats[:, :, 64:65] + stats[:, :, 96:97]
        own = own_rows[0][:, 0:1]
        highest = jnp.maximum(jnp.max(peak, axis=0), own)
        scale = jnp.exp(peak - highest[None])
        own_weight = jnp.exp(own - highest)
        own_round = own_weight.astype(BF16).astype(F32)
        total = jnp.sum(scale * den, axis=0) + own_weight
        weighted = jnp.sum(scale * num, axis=0) + own_round * own_rows[1]
        mixed = weighted / total
        head = lax.broadcasted_iota(jnp.int32, (NH, LANES), 0)
        its_lanes = lax.broadcasted_iota(jnp.int32, (NH, LANES), 1) == head * (LANES // NH)
        lam_rows = jnp.sum(jnp.where(its_lanes, own_rows[2][0:NH], 0.0), axis=1, keepdims=True)
        mixed = mixed[0:NH] - lam_rows * mixed[NH : 2 * NH]
        inv = lax.rsqrt(jnp.mean(mixed * mixed, axis=1, keepdims=True) + EPSILON)
        normed = mixed * inv * v_head_gain[...]
        head_row[...] = jnp.concatenate([normed, jnp.zeros((NH, LANES), F32)], axis=0).astype(BF16)
        share_row(2, head_row, head_all)

    take_all(2, att_out, short_rows, head_all)
    attended = as_lhs(head_all, NH)
    copies[8].wait()
    part = jnp.dot(attended, v_output[...], preferred_element_type=F32)
    second = (first + tp_sum(2, part)).astype(BF16).astype(F32)

    part = gated_units(1, second, v_gain3, v_gate2, v_up2, v_down2, copies[9:12])
    last = second + 0.5 * tp_sum(3, part)
    own_columns = lax.rem(LANES - t * columns, LANES)
    result[...] = pltpu.roll(last, own_columns, 1)[:, 0:columns].astype(BF16)


def on_device(KV, TP):
    def run(
        tokens,
        first_gain,
        first_gate,
        first_up,
        first_down,
        mixer_gain,
        w_query,
        w_key,
        w_value,
        w_output,
        lam_heads,
        head_gain,
        key_cache,
        value_cache,
        lengths,
        last_gain,
        last_gate,
        last_up,
        last_down,
    ):
        B, POS, NH, _ = key_cache.shape
        FB = first_gate.shape[1] // LANES
        FH = FB + 1
        HR = -(-FH // 8) * 8
        WIDTH = w_query.shape[0] * KV
        dims = (KV, TP, B, NH, FB, POS, WIDTH)
        far = pl.BlockSpec(memory_space=pl.ANY)
        smem = pl.BlockSpec(memory_space=pltpu.SMEM)
        flat_keys = key_cache.reshape(B, POS * NH, LANES)
        flat_values = value_cache.reshape(B, POS * NH, LANES)
        large = (first_gate, first_up, first_down, w_query, w_key, w_value, w_output)
        large += (flat_keys, flat_values, last_gate, last_up, last_down)
        return pl.pallas_call(
            functools.partial(layer_kernel, dims),
            out_shape=jax.ShapeDtypeStruct(tokens.shape, BF16),
            in_specs=[far] * 5 + [smem] * 2 + [far] * 12,
            out_specs=pl.BlockSpec(memory_space=pltpu.VMEM),
            scratch_shapes=[
                *(pltpu.VMEM(a.shape, a.dtype) for a in large),
                pltpu.VMEM(tokens.shape, BF16),
                *(pltpu.VMEM((1, LANES), F32) for _ in range(4)),
                pltpu.SemaphoreType.DMA((17,)),
                pltpu.VMEM((4, TP, B, LANES), BF16),
                pltpu.SemaphoreType.DMA((4,)),
                pltpu.SemaphoreType.DMA((4,)),
                pltpu.VMEM((max(2 * FH, 4 * NH) * B, LANES), F32),
                pltpu.VMEM((max(HR, 2 * NH) * B, LANES), F32),
                pltpu.VMEM((2, B, 2 * FH, LANES), BF16),
                pltpu.VMEM((2, KV, 2 * FH, LANES), BF16),
                pltpu.VMEM((B, 4 * NH, LANES), BF16),
                pltpu.VMEM((KV, 4 * NH, LANES), BF16),
                pltpu.VMEM((B, 4 * NH, LANES), BF16),
                pltpu.VMEM((KV, 4 * NH, LANES), BF16),
                pltpu.VMEM((2, HR, LANES), BF16),
                pltpu.VMEM((2, B, HR, LANES), BF16),
                pltpu.VMEM((2 * NH, LANES), BF16),
                pltpu.VMEM((B, 2 * NH, LANES), BF16),
                pltpu.VMEM((2 * NH, LANES), BF16),
                pltpu.VMEM((B, 2 * NH, LANES), BF16),
                pltpu.VMEM((3, 2 * NH, LANES), F32),
                pltpu.VMEM((KV, HR, LANES), BF16),
                pltpu.VMEM((KV, 2 * NH, LANES), BF16),
                pltpu.SemaphoreType.DMA((4,)),
                pltpu.SemaphoreType.DMA((4,)),
                pltpu.SemaphoreType.DMA((4,)),
                pltpu.SemaphoreType.DMA((4,)),
            ],
            compiler_params=pltpu.CompilerParams(collective_id=0, has_side_effects=True),
        )(
            tokens,
            first_gain.reshape(1, LANES),
            mixer_gain.reshape(1, LANES),
            last_gain.reshape(1, LANES),
            head_gain.reshape(1, LANES),
            lam_heads,
            lengths,
            first_gate,
            first_up,
            first_down,
            w_query,
            w_key,
            w_value,
            w_output,
            flat_keys,
            flat_values,
            last_gate,
            last_up,
            last_down,
        )

    return run


def solution(mesh):
    return jax.shard_map(
        on_device(mesh.shape["kv"], mesh.shape["tp"]),
        mesh=mesh,
        in_specs=(
            P(None, ("kv", "tp")),
            P("kv"),
            P("kv", "tp"),
            P("kv", "tp"),
            P("tp", "kv"),
            P("kv"),
            P("kv", "tp"),
            P("kv", "tp"),
            P("kv", "tp"),
            P("tp", "kv"),
            P("tp"),
            P(),
            P(None, "kv", "tp", None),
            P(None, "kv", "tp", None),
            P(),
            P("kv"),
            P("kv", "tp"),
            P("kv", "tp"),
            P("tp", "kv"),
        ),
        out_specs=P(None, ("kv", "tp")),
        check_vma=False,
    )
```

time: 95 us -> 76 us (0.80)
  Pallas kernels: 93.6 us -> 74.5 us
    pallas_call x1, Pallas kernels: 93.6 us -> 74.5 us  [run(): pl.pallas_call(functools.partial(layer_kernel, dims), out_shape=jax.Shape...]
where the time goes in v2:
time: 76 us; the launch traced here: 75.8 us
  Pallas kernels  74.5 us (98%)
  local copies, waits for them, and re-layouts  1.28 us (2%)
    pallas_call x1, Pallas kernels, run(): pl.pallas_call(functools.partial(layer_kernel, dims), out_shape=jax.Shape...  74.5 us

profile of v2, /device:TPU:1, one launch (start us, length us, event | category | flops | bytes accessed | tf_op | source)
XLA Modules:
  0.0 75.8 jit_solution(1141079586336867247)
XLA Ops:
  0.0 74.5 %shard_map.181 = bf16[16,16]{1,0:T(8,128)(2,1)} custom-call(bf16[16,16]{1,0:T(8,128)(2,1)} %tokens.1, f32[1,128]{1,0:T(1,128)} %bitcast.8, f32[1,128]{1,0:T(1,128)} %bitcast.9, f32[1,128]{1,0:T(1,128)} %bitcast.10, f32[1,128]{1,0:T(1,128)} %bitcast.11, f32[4]{0:T(128)} %lam.1, s32[16]{0:T(128)} %lengths.1, bf16[128,1408]{1,0:T(8,128)(2,1)} %first_gate.1, ...), custom_call_target="tpu_custom_call" | custom-call | tf_op jit(solution)/shard_map/pallas_call | solution.py:504
  74.5 1.3 %copy.21 = bf16[16,16]{1,0:T(8,128)(2,1)} copy(bf16[16,16]{1,0:T(8,128)(2,1)} %shard_map.181) | data formatting | bytes 1024
